TPU v7x, 128 devices: a whole 4x4x4 slice. The times are simulated.
128 devices in a mesh: sp: 64 (over z, y, x), tp: 2 (over core).
Axes of the slice: x: 4, y: 4, z: 4, core: 2. Of those that a mesh axis runs over, the one named last changes fastest.
Arguments:
- queries: bfloat16 [16384, 1024], P('sp', 'tp'), may hold values from -7 to 7
- keys: bfloat16 [16384, 256], P('sp', 'tp'), may hold values from -6 to 6
- values: bfloat16 [16384, 256], P('sp', 'tp'), may hold values from -6 to 6
- q_gain: float32 [64], replicated, may hold values from 0.5 to 5
- k_gain: float32 [64], replicated, may hold values from 0.5 to 5
- resid: bfloat16 [16384, 2048], P(('sp', 'tp')), may hold values from -6 to 6
- out_weight: bfloat16 [1024, 2048], P('tp'), may hold values from -0.1875 to 0.1875
- post_gain: float32 [2048], replicated, may hold values from 0.1 to 1.9
- ffn_gain: float32 [2048], replicated, may hold values from 0.1 to 1.9
- post_ffn_gain: float32 [2048], replicated, may hold values from 0.1 to 1.9
- gate_w: bfloat16 [64, 2048, 3584], P('sp', None, 'tp'), may hold values from -0.125 to 0.125
- up_w: bfloat16 [64, 2048, 3584], P('sp', None, 'tp'), may hold values from -0.125 to 0.125
- down_w: bfloat16 [64, 3584, 2048], P('sp', 'tp'), may hold values from -0.09375 to 0.09375
- route_ids: int32 [16384, 2], P(('sp', 'tp')), may hold values from 0 to 63, all different within a row; in each aligned block of 128 rows (0 to 127, 128 to 255, ...) at most 6 rows name the same one
- route_w: float32 [16384, 2], P(('sp', 'tp')), may hold values from 0.2 to 1
Outputs:
- layer_out: bfloat16 [16384, 2048], P(('sp', 'tp'))
Inputs may be any that keep to these rules, and one draw needn't show every extreme that they name: `route_ids`: each row names 2 different experts. In each aligned block of 128 rows (the rows of one device) no expert is named more than 6 times, a bound that some blocks reach.
All inputs are finite; a program needn't handle non-finite values.
Results may differ from a plain program's by a relative error of at most 0.017.
The roundings to bfloat16 on the way count: a program that leaves them out, or rounds other values in their place, can miss the bound.
Values may be sent and summed in bfloat16 or wider, within the bound.
A program may use at most 128 MiB of HBM per device.

v0:
```python
import jax
import jax.numpy as jnp
from jax import lax
from jax.experimental import pallas as pl
from jax.experimental.pallas import tpu as pltpu
from jax.sharding import PartitionSpec as P

HEAD_DIM = 64
GRID_W = 64


EPS = 1e-06
THETA = 10000.0


def qk_prepare(raw, gain, positions, head_count):
    count_rows = raw.shape[0]
    values32 = raw.astype(jnp.float32).reshape(count_rows, head_count, HEAD_DIM)
    normed = (
        values32 * lax.rsqrt(jnp.mean(values32 * values32, axis=-1, keepdims=True) + EPS) * gain
    )
    half_dim = HEAD_DIM // 2
    freqs = THETA ** (-jnp.arange(0, half_dim, 2, dtype=jnp.float32) / half_dim)
    grid_row = (positions // GRID_W).astype(jnp.float32)
    grid_col = (positions % GRID_W).astype(jnp.float32)
    angles = jnp.concatenate([grid_row[:, None] * freqs, grid_col[:, None] * freqs], axis=-1)
    cosine = jnp.cos(angles)[:, None, :]
    sine = jnp.sin(angles)[:, None, :]
    paired = normed.reshape(count_rows, head_count, half_dim, 2)
    first = paired[..., 0]
    second = paired[..., 1]
    turned = jnp.stack([first * cosine - second * sine, first * sine + second * cosine], axis=-1)
    return turned.reshape(count_rows, head_count * HEAD_DIM).astype(jnp.bfloat16)


def rms_scale(values32, gain):
    return values32 * lax.rsqrt(jnp.mean(values32 * values32, axis=-1, keepdims=True) + EPS) * gain


MESH_ID = pl.DeviceIdType.MESH
LIMIT = 2.0**100
QSCALE = 1.4426950408889634 / 8.0


def hops(d):
    return (0, 1, 2, 1)[d]


ORDER = sorted(range(64), key=lambda o: hops(o // 16) + hops(o // 4 % 4) + hops(o % 4))


def packed(start):
    words = []
    for g in range(16):
        w = 0
        for j in range(4):
            n = 4 * g + start + j
            w += (ORDER[n] if n < 64 else 0) * 64**j
        words.append(w)
    return words


def lookup(words, g):
    w = jnp.int32(words[0])
    for i in range(1, len(words)):
        w = jnp.where(g == i, jnp.int32(words[i]), w)
    return w


def pick(a, z, y, x):
    return jnp.where(a == 0, z, jnp.where(a == 1, y, x))


def source_of(offset, me):
    mz, my, mx = me // 16, (me // 4) % 4, me % 4
    cz = (mz + 4 - offset // 16) % 4
    cy = (my + 4 - (offset // 4) % 4) % 4
    cx = (mx + 4 - offset % 4) % 4
    return cz * 16 + cy * 4 + cx


def each_send(offset, me, act):
    mz, my, mx = me // 16, (me // 4) % 4, me % 4
    oz, oy, ox = offset // 16, (offset // 4) % 4, offset % 4
    src = source_of(offset, me)
    total = src // 16 + (src // 4) % 4 + src % 4
    kind, odd = total % 3, total % 2
    axes = [(kind + i) % 3 for i in range(3)]
    stride = [pick(a, 16, 4, 1) for a in axes]
    digit = [pick(a, oz, oy, ox) for a in axes]
    mine = [pick(a, mz, my, mx) for a in axes]

    def peer(i, step):
        return me + ((mine[i] + step) % 4 - mine[i]) * stride[i]

    none = offset == 0
    last = jnp.where(digit[2] > 0, 2, jnp.where(digit[1] > 0, 1, jnp.where(digit[0] > 0, 0, -1)))
    for i in range(3):

        @pl.when(i > last)
        def _():
            act(src, peer(i, 1), 2 * i)
            act(src, peer(i, 3), 2 * i + 1)

        @pl.when(jnp.logical_and(i == last, jnp.logical_and(digit[i] == 1, odd == 0)))
        def _():
            act(src, peer(i, 1), 2 * i)

        @pl.when(jnp.logical_and(i == last, jnp.logical_and(digit[i] == 3, odd == 1)))
        def _():
            act(src, peer(i, 3), 2 * i + 1)


def turned_heads(x, gain, cosine, sine):
    out = []
    for h in range(2):
        even, odd = x[64 * h : 64 * h + 32], x[64 * h + 32 : 64 * h + 64]
        squares = jnp.sum(even * even, axis=0, keepdims=True) + jnp.sum(odd * odd, axis=0, keepdims=True)
        scale = lax.rsqrt(squares * (1.0 / 64.0) + EPS)
        even, odd = even * scale * gain[0:32], odd * scale * gain[32:64]
        out.append(jnp.concatenate([even * cosine - odd * sine, even * sine + odd * cosine], axis=0))
    return out


def attention_kernel(
    q_ref, k_ref, v_ref, gains_ref, trig_ref, ow_ref, o_ref, den_ref, kv_out, ow_out,
    qt, top, acc, kv, send_sem, recv_sem, out_sem, swap_sem,
):
    me, core = lax.axis_index("sp"), lax.axis_index("tp")
    mz, my, mx = me // 16, (me // 4) % 4, me % 4
    barrier = pltpu.get_barrier_semaphore()
    for stride, c in ((16, mz), (4, my), (1, mx)):
        for step in (1, 3):
            to = me + ((c + step) % 4 - c) * stride
            pl.semaphore_signal(barrier, inc=1, device_id=(to, core), device_id_type=MESH_ID)
    pl.semaphore_signal(barrier, inc=1, device_id=(me, 1 - core), device_id_type=MESH_ID)

    row = lax.broadcasted_iota(jnp.int32, (128, 128), 0)
    col = lax.broadcasted_iota(jnp.int32, (128, 128), 1)
    within = row % 64
    wanted = (row // 64) * 64 + 2 * (within % 32) + within // 32
    order = (col == wanted).astype(jnp.float32).astype(jnp.bfloat16)
    same = (col == row).astype(jnp.float32).astype(jnp.bfloat16)
    nt = (((1,), (1,)), ((), ()))
    cosine, sine = trig_ref[0:32, :], trig_ref[32:64, :]
    kt = turned_heads(
        lax.dot_general(order, k_ref[...], nt, preferred_element_type=jnp.float32),
        gains_ref[64:128, :], cosine, sine,
    )
    kv[me, 0:256, :] = jnp.concatenate(kt, axis=0).T.astype(jnp.bfloat16)
    vt = lax.dot_general(same, v_ref[...], nt, preferred_element_type=jnp.float32).astype(jnp.bfloat16)
    kv[me, 256:384, :] = vt[:, 0:128]
    kv[me, 384:512, :] = vt[:, 128:256]

    qt[...] = jnp.zeros_like(qt)
    for j in range(4):
        heads = turned_heads(
            lax.dot_general(
                order, q_ref[:, 128 * j : 128 * j + 128], nt, preferred_element_type=jnp.float32
            ),
            gains_ref[0:64, :], cosine, sine,
        )
        for i in range(2):
            scaled = heads[i].astype(jnp.bfloat16).astype(jnp.float32) * QSCALE
            high = scaled.astype(jnp.bfloat16)
            low = (scaled - high.astype(jnp.float32)).astype(jnp.bfloat16)
            at, to = pl.ds((2 * j + i) * 256, 256), 64 * (j // 2)
            qt[to : to + 64, at] = high
            qt[128 + to : 192 + to, at] = low

    pl.semaphore_wait(barrier, 7)

    def copy(src, peer, slot):
        return pltpu.make_async_remote_copy(
            src_ref=kv.at[src], dst_ref=kv.at[src],
            send_sem=send_sem.at[src, slot], recv_sem=recv_sem.at[src],
            device_id=(peer, core), device_id_type=MESH_ID,
        )

    def start(src, peer, slot):
        copy(src, peer, slot).start()

    def finish(src, peer, slot):
        copy(src, peer, slot).wait_send()

    def take(offset):
        src = source_of(offset, me)
        copy(src, me, 0).wait_recv()
        each_send(offset, me, start)

    each_send(jnp.int32(0), me, start)
    swap = pltpu.make_async_remote_copy(
        src_ref=ow_ref, dst_ref=ow_out, send_sem=swap_sem.at[0], recv_sem=swap_sem.at[1],
        device_id=(me, 1 - core), device_id_type=MESH_ID,
    )
    swap.start()

    own = kv[me, 0:256, :]
    own = jnp.concatenate([own, own], axis=1)
    for t in range(4):
        at = pl.ds(t * 512, 512)
        s = jnp.dot(own, qt[:, at], preferred_element_type=jnp.float32)
        top[:, at] = jnp.broadcast_to(jnp.max(s, axis=0, keepdims=True), (8, 512))
    acc[...] = jnp.zeros_like(acc)
    ones = jnp.ones((16, 1024), jnp.bfloat16)
    for n in range(1, 3):
        take(jnp.int32(ORDER[n]))

    first, ahead = packed(0), packed(3)

    def group(g, carry):
        coming = lookup(ahead, g)
        for j in range(4):

            @pl.when(4 * g + 3 + j < 64)
            def _():
                take((coming // 64**j) % 64)

        now = lookup(first, g)
        srcs = [source_of((now // 64**j) % 64, me) for j in range(4)]
        for s in srcs:
            pltpu.make_async_copy(kv.at[s], kv_out.at[s], out_sem.at[s]).start()
        kk = jnp.concatenate([kv[s, 0:256, :] for s in srcs], axis=0)
        kk = jnp.concatenate([kk, kk], axis=1)
        vt = jnp.concatenate([kv[s, a : a + 128, :] for s in srcs for a in (256, 384)], axis=1)
        va = [jnp.concatenate([vt[64 * h : 64 * h + 64], ones], axis=0) for h in range(2)]
        for t in range(4):
            at = pl.ds(t * 512, 512)
            s = jnp.dot(kk, qt[:, at], preferred_element_type=jnp.float32)
            p = jnp.exp2(s - top[0:1, at]).astype(jnp.bfloat16)
            acc[:, at] += jnp.dot(va[t // 2], p, preferred_element_type=jnp.float32)
        return carry

    lax.fori_loop(0, 16, group, 0)

    for j in range(4):
        parts = []
        for i in range(2):
            at = pl.ds((2 * j + i) * 256, 256)
            parts.append(acc[0:64, at] / acc[64:65, at])
        o_ref[:, 128 * j : 128 * j + 128] = jnp.concatenate(parts, axis=0).T.astype(jnp.bfloat16)
    den_ref[...] = jnp.broadcast_to(jnp.max(acc[64:65, :]), (8, 128))

    def drain(g, carry):
        now = lookup(first, g)
        for j in range(4):
            offset = (now // 64**j) % 64
            each_send(offset, me, finish)
            s = source_of(offset, me)
            pltpu.make_async_copy(kv.at[s], kv_out.at[s], out_sem.at[s]).wait()
        return carry

    lax.fori_loop(0, 16, drain, 0)
    swap.wait()


def attention(queries, keys, values, q_gain, k_gain, out_weight):
    me = lax.axis_index("sp")
    half = HEAD_DIM // 2
    freqs = THETA ** (-jnp.arange(0, half, 2, dtype=jnp.float32) / half)
    positions = me * 256 + jnp.arange(256, dtype=jnp.int32)
    grid_row = (positions // GRID_W).astype(jnp.float32)
    grid_col = (positions % GRID_W).astype(jnp.float32)
    angles = jnp.concatenate([freqs[:, None] * grid_row, freqs[:, None] * grid_col], axis=0)
    trig = jnp.concatenate([jnp.cos(angles), jnp.sin(angles)], axis=0)
    pairs = [g.reshape(32, 2).T.reshape(64) for g in (q_gain, k_gain)]
    gains = jnp.broadcast_to(jnp.concatenate(pairs)[:, None], (128, 256))
    vmem, hbm = pl.BlockSpec(memory_space=pltpu.VMEM), pl.BlockSpec(memory_space=pltpu.HBM)
    return pl.pallas_call(
        attention_kernel,
        out_shape=(
            jax.ShapeDtypeStruct((256, 512), jnp.bfloat16),
            jax.ShapeDtypeStruct((8, 128), jnp.float32),
            jax.ShapeDtypeStruct((64, 512, 128), jnp.bfloat16),
            jax.ShapeDtypeStruct((512, 2048), jnp.bfloat16),
        ),
        in_specs=[vmem] * 5 + [hbm],
        out_specs=(vmem, vmem, hbm, hbm),
        scratch_shapes=[
            pltpu.VMEM((256, 2048), jnp.bfloat16),
            pltpu.VMEM((8, 2048), jnp.float32),
            pltpu.VMEM((80, 2048), jnp.float32),
            pltpu.VMEM((64, 512, 128), jnp.bfloat16),
            pltpu.SemaphoreType.DMA((64, 6)),
            pltpu.SemaphoreType.DMA((64,)),
            pltpu.SemaphoreType.DMA((64,)),
            pltpu.SemaphoreType.DMA((2,)),
        ],
        compiler_params=pltpu.CompilerParams(
            collective_id=0, has_side_effects=True, vmem_limit_bytes=56 << 20
        ),
        cost_estimate=pl.CostEstimate(flops=17_000_000_000, bytes_accessed=9_000_000, transcendentals=0),
        name="attention",
    )(queries, keys, values, gains, trig, out_weight)


def attention_again(queries, q_gain, kv):
    me = lax.axis_index("sp")
    positions = me * 256 + jnp.arange(256, dtype=jnp.int32)
    qn = qk_prepare(queries, q_gain, positions, 8).reshape(256, 2, 4, 32, 2)
    qn = jnp.swapaxes(qn, -1, -2).reshape(256, 2, 4, 64)
    k = kv[:, 0:256].reshape(64, 256, 2, 64)
    v = jnp.concatenate([kv[:, 256:384], kv[:, 384:512]], axis=2).reshape(64, 2, 64, 256)

    def scores_of(kb):
        return jnp.einsum("qhgd,khd->hgqk", qn, kb, preferred_element_type=jnp.float32) * 0.125

    def largest(m, kb):
        return jnp.maximum(m, jnp.max(scores_of(kb), axis=-1)), None

    top, _ = lax.scan(largest, jnp.full((2, 4, 256), -1e30, jnp.float32), k)

    def add(carry, block):
        total, summed = carry
        kb, vb = block
        ex = jnp.exp(scores_of(kb) - top[..., None])
        summed += jnp.einsum(
            "hgqk,hdk->hgqd", ex.astype(jnp.bfloat16), vb, preferred_element_type=jnp.float32
        )
        return (total + jnp.sum(ex, axis=-1), summed), None

    zero = (jnp.zeros((2, 4, 256), jnp.float32), jnp.zeros((2, 4, 256, 64), jnp.float32))
    (total, summed), _ = lax.scan(add, zero, (k, v))
    out = jnp.transpose(summed / total[..., None], (2, 0, 1, 3))
    return out.reshape(256, 512).astype(jnp.bfloat16)


SLOTS = 6
PLANE = 16 * SLOTS


def experts_kernel(
    att_ref, resid_ref, gains_ref, ids_ref, rw_ref, ow_ref, owp_ref, gate_hbm, up_hbm, down_hbm, o_ref,
    ow, owp, gate, up, down, att_in, hidden, out, arr, x, inner, part, part_out, part_in, total, ret, combined, tiles,
    w_sem, a_sem, d_send, d_recv, f_send, f_recv, p_send, p_recv, r_send, r_recv,
):
    me, core = lax.axis_index("sp"), lax.axis_index("tp")
    mz, mq = me // 16, me % 16
    other = 1 - core
    f32, bf16 = jnp.float32, jnp.bfloat16

    barrier = pltpu.get_barrier_semaphore()

    def greet(i, carry):
        pl.semaphore_signal(barrier, inc=1, device_id=((me + i) % 64, core), device_id_type=MESH_ID)
        return carry

    lax.fori_loop(1, 64, greet, 0)
    pl.semaphore_signal(barrier, inc=1, device_id=(me, other), device_id_type=MESH_ID)
    loads = [
        pltpu.make_async_copy(src, dst, w_sem.at[i])
        for i, (src, dst) in enumerate(
            ((ow_ref, ow), (owp_ref, owp), (gate_hbm.at[0], gate), (up_hbm.at[0], up), (down_hbm.at[0], down))
        )
    ]
    for load in loads:
        load.start()

    lane = lax.broadcasted_iota(jnp.int32, (128, 64), 1)
    chosen = [(ids_ref[:, k : k + 1] == lane).astype(f32) for k in range(2)]
    below = (
        lax.broadcasted_iota(jnp.int32, (128, 128), 1) < lax.broadcasted_iota(jnp.int32, (128, 128), 0)
    ).astype(f32).astype(bf16)
    earlier = [jnp.dot(below, c.astype(bf16), preferred_element_type=f32) for c in chosen]
    earlier[1] = earlier[1] + jnp.sum(chosen[0], axis=0, keepdims=True)
    slot = [
        ids_ref[:, k : k + 1] * SLOTS
        + jnp.sum(earlier[k] * chosen[k], axis=1, keepdims=True).astype(jnp.int32)
        for k in range(2)
    ]
    within = lax.broadcasted_iota(jnp.int32, (128, PLANE), 1)

    def offset_of(j):
        return jnp.where(j == 2, 3, jnp.where(j == 3, 2, j))

    pl.semaphore_wait(barrier, 64)

    here = pl.ds(pl.multiple_of(core * 128, 128), 128)
    there = pl.ds(pl.multiple_of(other * 128, 128), 128)
    swap = pltpu.make_async_remote_copy(
        src_ref=att_ref.at[there], dst_ref=att_in, send_sem=a_sem.at[0], recv_sem=a_sem.at[1],
        device_id=(me, other), device_id_type=MESH_ID,
    )
    swap.start()
    loads[0].wait()
    mixed = jnp.dot(att_ref[here, :], ow[...], preferred_element_type=f32)
    loads[1].wait()
    swap.wait()
    mixed = mixed + jnp.dot(att_in[...], owp[...], preferred_element_type=f32)
    state = (resid_ref[...].astype(f32) + rms_scale(mixed, gains_ref[0:1, :])).astype(bf16)
    hidden[...] = state
    normed = rms_scale(state.astype(f32), gains_ref[1:2, :]).astype(bf16)

    def block(ref, s):
        return ref.at[pl.ds(s * SLOTS, SLOTS)]

    def there_copy(s):
        return pltpu.make_async_remote_copy(
            src_ref=block(out, s), dst_ref=block(arr.at[core], me), send_sem=d_send.at[s], recv_sem=d_recv.at[me],
            device_id=(s, core), device_id_type=MESH_ID,
        )

    def arrival(s):
        return pltpu.make_async_remote_copy(
            src_ref=block(out, s), dst_ref=block(arr.at[core], s), send_sem=d_send.at[s], recv_sem=d_recv.at[s],
            device_id=(s, core), device_id_type=MESH_ID,
        )

    def back_copy(s):
        return pltpu.make_async_remote_copy(
            src_ref=block(total, s), dst_ref=block(ret, me), send_sem=r_send.at[s], recv_sem=r_recv.at[me],
            device_id=(s, core), device_id_type=MESH_ID,
        )

    def back_arrival(s):
        return pltpu.make_async_remote_copy(
            src_ref=block(total, s), dst_ref=block(ret, s), send_sem=r_send.at[s], recv_sem=r_recv.at[s],
            device_id=(s, core), device_id_type=MESH_ID,
        )

    def for_plane(z, first, act):
        def step(i, carry):
            act(z * 16 + (mq + i) % 16)
            return carry

        lax.fori_loop(first, 16, step, 0)

    def skip(j):
        return jnp.where(j == 0, 1, 0)

    def dispatch(j, carry):
        z = (mz + offset_of(j)) % 4
        place = within + z * PLANE
        picked = ((slot[0] == place).astype(f32) + (slot[1] == place).astype(f32)).astype(bf16)
        rows = lax.dot_general(picked, normed, (((0,), (0,)), ((), ())), preferred_element_type=f32)
        tiles[...] = rows.astype(bf16).reshape(PLANE, 16, 128)
        out[pl.ds(z * PLANE, PLANE)] = tiles[...]
        for_plane(z, skip(j), lambda s: there_copy(s).start())
        return carry

    lax.fori_loop(0, 4, dispatch, 0)
    arr[core, pl.ds(me * SLOTS, SLOTS)] = out[pl.ds(me * SLOTS, SLOTS)]
    for load in loads[2:]:
        load.wait()

    def forward(j):
        z = (mz + 4 - offset_of(j)) % 4
        rows = pl.ds(z * PLANE, PLANE)
        return pltpu.make_async_remote_copy(
            src_ref=arr.at[core, rows], dst_ref=arr.at[core, rows], send_sem=f_send.at[j], recv_sem=f_recv.at[j],
            device_id=(me, other), device_id_type=MESH_ID,
        )

    def partial(j):
        return pltpu.make_async_remote_copy(
            src_ref=part_out.at[j], dst_ref=part_in.at[j], send_sem=p_send.at[j], recv_sem=p_recv.at[j],
            device_id=(me, other), device_id_type=MESH_ID,
        )

    def finish(j):
        z = (mz + 4 - offset_of(j)) % 4
        partial(j).wait_recv()
        rows = (part[j].astype(f32) + part_in[j].astype(f32)).astype(bf16)
        tiles[...] = rows.reshape(PLANE, 16, 128)
        total[pl.ds(z * PLANE, PLANE)] = tiles[...]

        @pl.when(j == 0)
        def _():
            ret[pl.ds(me * SLOTS, SLOTS)] = total[pl.ds(me * SLOTS, SLOTS)]

        for_plane(z, skip(j), lambda s: back_copy(s).start())

    def chunk(j, carry):
        z = (mz + 4 - offset_of(j)) % 4
        rows = pl.ds(z * PLANE, PLANE)
        for_plane(z, skip(j), lambda s: arrival(s).wait_recv())
        forward(j).start()
        tiles[...] = arr[core, rows]
        x[0:PLANE, :] = tiles[...].reshape(PLANE, 2048)
        forward(j).wait_recv()
        tiles[...] = arr[other, rows]
        x[PLANE : 2 * PLANE, :] = tiles[...].reshape(PLANE, 2048)
        for n in range(7):
            at = pl.ds(n * 256, 256)
            g = jnp.dot(x[...], gate[:, at], preferred_element_type=f32)
            u = jnp.dot(x[...], up[:, at], preferred_element_type=f32)
            inner[:, at] = (g / (1.0 + jnp.exp(-g)) * u).astype(bf16)
        for n in range(8):
            at = pl.ds(n * 256, 256)
            y = jnp.dot(inner[...], down[:, at], preferred_element_type=f32).astype(bf16)
            part[j, :, at] = y[0:PLANE]
            part_out[j, :, at] = y[PLANE : 2 * PLANE]

        partial(j).start()

        @pl.when(j > 0)
        def _():
            finish(j - 1)

        return carry

    lax.fori_loop(0, 4, chunk, 0)
    finish(jnp.int32(3))

    combined[...] = jnp.zeros_like(combined)

    def collect(j, carry):
        z = (mz + offset_of(j)) % 4
        for_plane(z, skip(j), lambda s: back_arrival(s).wait_recv())
        place = within + z * PLANE
        weight = jnp.where(slot[0] == place, rw_ref[:, 0:1], 0.0) + jnp.where(slot[1] == place, rw_ref[:, 1:2], 0.0)
        high = weight.astype(bf16)
        low = (weight - high.astype(f32)).astype(bf16)
        tiles[...] = ret[pl.ds(z * PLANE, PLANE)]
        rows = tiles[...].reshape(PLANE, 2048)
        combined[...] += jnp.dot(high, rows, preferred_element_type=f32) + jnp.dot(
            low, rows, preferred_element_type=f32
        )
        return carry

    lax.fori_loop(0, 4, collect, 0)
    o_ref[...] = (hidden[...].astype(f32) + rms_scale(combined[...], gains_ref[2:3, :])).astype(bf16)

    swap_sends = [forward, partial]

    def drain(j, carry):
        for_plane(j, jnp.where(j == mz, 1, 0), lambda s: there_copy(s).wait_send())
        for_plane(j, jnp.where(j == mz, 1, 0), lambda s: back_copy(s).wait_send())
        for make in swap_sends:
            make(j).wait_send()
        return carry

    lax.fori_loop(0, 4, drain, 0)


def experts(attended, resid, gains, route_ids, route_w, out_weight, out_weight_other, gate_w, up_w, down_w):
    vmem, hbm = pl.BlockSpec(memory_space=pltpu.VMEM), pl.BlockSpec(memory_space=pltpu.HBM)
    bf16, f32, dma = jnp.bfloat16, jnp.float32, pltpu.SemaphoreType.DMA
    return pl.pallas_call(
        experts_kernel,
        out_shape=jax.ShapeDtypeStruct((128, 2048), bf16),
        in_specs=[vmem] * 5 + [hbm] * 5,
        out_specs=vmem,
        scratch_shapes=[
            pltpu.VMEM((512, 2048), bf16),
            pltpu.VMEM((512, 2048), bf16),
            pltpu.VMEM((2048, 1792), bf16),
            pltpu.VMEM((2048, 1792), bf16),
            pltpu.VMEM((1792, 2048), bf16),
            pltpu.VMEM((128, 512), bf16),
            pltpu.VMEM((128, 2048), bf16),
            pltpu.VMEM((384, 16, 128), bf16),
            pltpu.VMEM((2, 384, 16, 128), bf16),
            pltpu.VMEM((2 * PLANE, 2048), bf16),
            pltpu.VMEM((2 * PLANE, 1792), bf16),
            pltpu.VMEM((4, PLANE, 2048), bf16),
            pltpu.VMEM((4, PLANE, 2048), bf16),
            pltpu.VMEM((4, PLANE, 2048), bf16),
            pltpu.VMEM((384, 16, 128), bf16),
            pltpu.VMEM((384, 16, 128), bf16),
            pltpu.VMEM((128, 2048), f32),
            pltpu.VMEM((PLANE, 16, 128), bf16),
            dma((5,)), dma((2,)), dma((64,)), dma((64,)), dma((4,)), dma((4,)), dma((4,)), dma((4,)),
            dma((64,)), dma((64,)),
        ],
        compiler_params=pltpu.CompilerParams(
            collective_id=1, has_side_effects=True, vmem_limit_bytes=60 << 20
        ),
        cost_estimate=pl.CostEstimate(flops=20_000_000_000, bytes_accessed=28_000_000, transcendentals=0),
        name="experts",
    )(attended, resid, gains, route_ids, route_w, out_weight, out_weight_other, gate_w, up_w, down_w)


def per_device(
    queries,
    keys,
    values,
    q_gain,
    k_gain,
    resid,
    out_weight,
    post_gain,
    ffn_gain,
    post_ffn_gain,
    gate_w,
    up_w,
    down_w,
    route_ids,
    route_w,
):
    attended, den, kv, out_weight_other = attention(queries, keys, values, q_gain, k_gain, out_weight)
    attended = lax.cond(
        den[0, 0] < LIMIT,
        lambda: attended,
        lambda: attention_again(queries, q_gain, kv),
    )
    gains = jnp.concatenate([post_gain[None], ffn_gain[None], post_ffn_gain[None], jnp.zeros((5, 2048), jnp.float32)])
    return experts(
        attended, resid, gains, route_ids, route_w, out_weight, out_weight_other, gate_w, up_w, down_w
    )


def solution(mesh):
    in_specs = (
        P("sp", "tp"),
        P("sp", "tp"),
        P("sp", "tp"),
        P(),
        P(),
        P(("sp", "tp"), None),
        P("tp", None),
        P(),
        P(),
        P(),
        P("sp", None, "tp"),
        P("sp", None, "tp"),
        P("sp", "tp", None),
        P(("sp", "tp"), None),
        P(("sp", "tp"), None),
    )
    out_specs = P(("sp", "tp"), None)
    return jax.shard_map(
        per_device, mesh=mesh, in_specs=in_specs, out_specs=out_specs, check_vma=False
    )
```

profile of v0, /device:TPU:1, one launch (start us, length us, event | category | flops | bytes accessed | tf_op | source)
XLA Modules:
  0.0 153.9 jit_solution(15987356708276468762)
XLA Ops:
  0.0 0.1 broadcast_multiply_fusion.3
  0.1 0.1 fusion.23
  0.2 0.6 pad_maximum_fusion.3.trig_ref
  0.9 0.7 reshape.187
  1.6 0.1 copy.28
  1.7 0.1 reshape.188
  1.8 0.8 reshape.189
  2.6 0.1 copy.29
  2.6 0.1 reshape.190
  2.7 0.1 pad_maximum_fusion.5
  2.8 0.8 broadcast_in_dim.10.gains_ref
  3.6 0.0 copy-start
  3.6 0.0 copy-start.4
  3.6 70.3 %attention.1 = (bf16[256,512]{1,0:T(8,128)(2,1)S(1)}, f32[8,128]{1,0:T(8,128)}, bf16[64,512,128]{2,1,0:T(8,128)(2,1)}, bf16[512,2048]{1,0:T(8,128)(2,1)}) custom-call(bf16[256,512]{1,0:T(8,128)(2,1)} %q_ref.1, bf16[256,128]{1,0:T(8,128)(2,1)} %k_ref.1, bf16[256,128]{1,0:T(8,128)(2,1)} %v_ref.1, f32[128,256]{1,0:T(8,128)} %broadcast_in_dim.10.gains_ref, ...), custom_call_target="tpu_custom_call" | custom-call | flops 16999999488 | bytes 9000000 | tf_op jit(solution)/shard_map/attention/pallas_call | solution.py:269
  73.9 1.2 slice.18
  75.7 0.0 copy-done
  75.7 0.0 copy-done.4
  75.8 0.0 copy-start.1
  75.8 0.0 copy-start.2
  75.8 0.0 copy-start.3
  75.8 0.0 copy-start.5
  75.8 0.0 copy-start.6
  75.8 0.2 conditional.1
  76.0 0.1 pad.9.clone
  76.1 0.4 copy-done.1
  76.5 0.0 copy-done.2
  76.5 0.0 copy-done.3
  76.5 0.7 maximum_maximum_fusion.gains_ref
  77.2 0.0 copy-done.5
  77.2 0.7 copy.33.ids_ref
  77.9 0.0 copy-done.6
  77.9 0.7 copy.34.rw_ref
  78.7 73.4 %experts.1 = bf16[128,2048]{1,0:T(8,128)(2,1)} custom-call(bf16[256,512]{1,0:T(8,128)(2,1)S(1)} %get-tuple-element.128.att_ref, bf16[128,2048]{1,0:T(8,128)(2,1)} %resid_ref.1, f32[8,2048]{1,0:T(8,128)} %maximum_maximum_fusion.gains_ref, s32[128,2]{1,0:T(8,128)} %copy.33.ids_ref, f32[128,2]{1,0:T(8,128)} %copy.34.rw_ref, bf16[512,2048]{1,0:T(8,128)(2,1)} %ow_ref.3, ...), custom_call_target="tpu_custom_call" | custom-call | flops 20000000000 | bytes 28000000 | tf_op jit(solution)/shard_map/experts/pallas_call | solution.py:539
  152.1 1.9 %copy.59 = bf16[128,2048]{1,0:T(8,128)(2,1)} copy(bf16[128,2048]{1,0:T(8,128)(2,1)} %experts.1) | data formatting | bytes 1048576
  (3 shorter events, 0.0 us)
Async XLA Ops:
  3.6 72.2 %copy-start = (bf16[256,512]{1,0:T(8,128)(2,1)S(1)}, bf16[256,512]{1,0:T(8,128)(2,1)}, u32[]{:S(2)}) copy-start(bf16[256,512]{1,0:T(8,128)(2,1)} %q_ref.1) | copy-start | bytes 786436
  3.6 72.2 %copy-start.4 = (f32[64]{0:T(128)S(1)}, f32[64]{0:T(128)}, u32[]{:S(2)}) copy-start(f32[64]{0:T(128)} %param.24) | copy-start | bytes 772
  75.8 0.7 copy-start.1
  75.8 0.7 copy-start.2
  75.8 0.7 copy-start.3
  75.8 1.4 copy-start.5
  75.8 2.1 %copy-start.6 = (f32[128,2]{0,1:T(2,128)S(1)}, f32[128,2]{0,1:T(2,128)}, u32[]{:S(2)}) copy-start(f32[128,2]{0,1:T(2,128)} %param.35) | copy-start | bytes 3076
where the time goes:
time: 155 us; the launch traced here: 154 us
  Pallas kernels  144 us (93%)
  local copies, waits for them, and re-layouts  7.62 us (5%)
  other arithmetic  1.65 us (1%)
    pallas_call x1, Pallas kernels, experts(): pl.pallas_call(experts_kernel, out_shape=jax.ShapeDtypeStruct((128, 2048)...  73.4 us
    pallas_call x1, Pallas kernels, attention(): pl.pallas_call(attention_kernel, out_shape=(jax.ShapeDtypeStruct((256, 51...  70.3 us
    unnamed x17, local copies, waits for them, and re-layouts  3.78 us

commit v1 on v0

v1 whole, which is shorter than its diff:
```python
import jax
import jax.numpy as jnp
from jax import lax
from jax.experimental import pallas as pl
from jax.experimental.pallas import tpu as pltpu
from jax.sharding import PartitionSpec as P

HEAD_DIM = 64
GRID_W = 64


EPS = 1e-06
THETA = 10000.0


def qk_prepare(raw, gain, positions, head_count):
    count_rows = raw.shape[0]
    values32 = raw.astype(jnp.float32).reshape(count_rows, head_count, HEAD_DIM)
    normed = (
        values32 * lax.rsqrt(jnp.mean(values32 * values32, axis=-1, keepdims=True) + EPS) * gain
    )
    half_dim = HEAD_DIM // 2
    freqs = THETA ** (-jnp.arange(0, half_dim, 2, dtype=jnp.float32) / half_dim)
    grid_row = (positions // GRID_W).astype(jnp.float32)
    grid_col = (positions % GRID_W).astype(jnp.float32)
    angles = jnp.concatenate([grid_row[:, None] * freqs, grid_col[:, None] * freqs], axis=-1)
    cosine = jnp.cos(angles)[:, None, :]
    sine = jnp.sin(angles)[:, None, :]
    paired = normed.reshape(count_rows, head_count, half_dim, 2)
    first = paired[..., 0]
    second = paired[..., 1]
    turned = jnp.stack([first * cosine - second * sine, first * sine + second * cosine], axis=-1)
    return turned.reshape(count_rows, head_count * HEAD_DIM).astype(jnp.bfloat16)


def rms_scale(values32, gain):
    return values32 * lax.rsqrt(jnp.mean(values32 * values32, axis=-1, keepdims=True) + EPS) * gain


MESH_ID = pl.DeviceIdType.MESH
LIMIT = 2.0**100
QSCALE = 1.4426950408889634 / 8.0
ORDER = [0, 12, 48, 4, 16, 3, 1, 60, 28, 8, 52, 15, 32, 19, 2, 51, 5, 7, 20, 17, 13, 49, 56, 11, 24, 18, 35, 21, 6, 29, 36, 50, 55, 44, 23, 9, 33, 14, 61, 63, 25, 53, 59, 39, 45, 40, 10, 62, 34, 22, 27, 47, 41, 58, 57, 30, 38, 54, 43, 37, 31, 26, 46, 42]
PARTS = ((0, 176), (176, 176), (352, 160))


def digits(offset):
    return (offset // 16, offset // 4 % 4, offset % 4)


def onward(offset, part):
    place = digits(offset)
    axes = [(part + i) % 3 for i in range(3)]
    last = max([i for i in range(3) if place[axes[i]]], default=-1)
    out = []
    if last >= 0:
        came = place[axes[last]]
        if came == (1, 3)[(sum(place) - came + part) % 2]:
            out.append((axes[last], came))
    for axis in axes[last + 1 :]:
        out += [(axis, 1), (axis, 3)]
    return out


def relay_plan():
    plan = [[(o, r) for r in range(3) for o in ORDER[1:7]]]
    for g in range(1, 16):
        plan.append([(o, r) for o in ORDER[4 * g + 3 : 4 * g + 7] for r in range(3)])
    return plan


def packed():
    return [sum(ORDER[4 * g + j] * 64**j for j in range(4)) for g in range(16)]


def lookup(words, g):
    w = jnp.int32(words[0])
    for i in range(1, len(words)):
        w = jnp.where(g == i, jnp.int32(words[i]), w)
    return w


def source_of(offset, me):
    cz = (me // 16 + 4 - offset // 16) % 4
    cy = ((me // 4) % 4 + 4 - (offset // 4) % 4) % 4
    cx = (me % 4 + 4 - offset % 4) % 4
    return cz * 16 + cy * 4 + cx


def turned_heads(x, gain, cosine, sine):
    out = []
    for h in range(2):
        even, odd = x[64 * h : 64 * h + 32], x[64 * h + 32 : 64 * h + 64]
        squares = jnp.sum(even * even, axis=0, keepdims=True) + jnp.sum(odd * odd, axis=0, keepdims=True)
        scale = lax.rsqrt(squares * (1.0 / 64.0) + EPS)
        even, odd = even * scale * gain[0:32], odd * scale * gain[32:64]
        out.append(jnp.concatenate([even * cosine - odd * sine, even * sine + odd * cosine], axis=0))
    return out


def attention_kernel(
    q_ref, k_ref, v_ref, qg_ref, kg_ref, ow_ref, o_ref, den_ref, kv_out, ow_out,
    qt, top, acc, kv, send_sem, recv_sem, out_sem, swap_sem,
):
    me, core = lax.axis_index("sp"), lax.axis_index("tp")
    coords = (me // 16, (me // 4) % 4, me % 4)
    peers = {
        (axis, step): me + ((coords[axis] + step) % 4 - coords[axis]) * (16, 4, 1)[axis]
        for axis in range(3)
        for step in (1, 3)
    }
    barrier = pltpu.get_barrier_semaphore()
    for to in peers.values():
        pl.semaphore_signal(barrier, inc=1, device_id=(to, core), device_id_type=MESH_ID)
    pl.semaphore_signal(barrier, inc=1, device_id=(me, 1 - core), device_id_type=MESH_ID)

    row = lax.broadcasted_iota(jnp.int32, (128, 128), 0)
    col = lax.broadcasted_iota(jnp.int32, (128, 128), 1)
    within = row % 64
    wanted = (row // 64) * 64 + 2 * (within % 32) + within // 32
    order = (col == wanted).astype(jnp.float32).astype(jnp.bfloat16)
    same = (col == row).astype(jnp.float32).astype(jnp.bfloat16)
    nt = (((1,), (1,)), ((), ()))

    pair = lax.broadcasted_iota(jnp.int32, (32, 256), 0)
    token = lax.broadcasted_iota(jnp.int32, (32, 256), 1)
    freq = jnp.zeros((32, 256), jnp.float32)
    for i in range(16):
        freq = jnp.where(pair % 16 == i, jnp.float32(THETA ** (-i / 16.0)), freq)
    where = jnp.where(pair < 16, me * 4 + token // 64, token % 64)
    angle = where.astype(jnp.float32) * freq
    cosine, sine = jnp.cos(angle), jnp.sin(angle)

    def column(ref):
        return jnp.sum(jnp.where((col == wanted)[0:64, 0:64], ref[...], 0.0), axis=1, keepdims=True)

    kt = turned_heads(
        lax.dot_general(order, k_ref[...], nt, preferred_element_type=jnp.float32), column(kg_ref), cosine, sine
    )
    kv[me, 0:256, :] = jnp.concatenate(kt, axis=0).T.astype(jnp.bfloat16)
    vt = lax.dot_general(same, v_ref[...], nt, preferred_element_type=jnp.float32).astype(jnp.bfloat16)
    kv[me, 256:384, :] = vt[:, 0:128]
    kv[me, 384:512, :] = vt[:, 128:256]

    pl.semaphore_wait(barrier, 7)

    sends = [0, 0, 0]

    def copy(src, part, to, number):
        rows = pl.ds(*PARTS[part])
        return pltpu.make_async_remote_copy(
            src_ref=kv.at[src, rows], dst_ref=kv.at[src, rows],
            send_sem=send_sem.at[part, number], recv_sem=recv_sem.at[part, src],
            device_id=(to, core), device_id_type=MESH_ID,
        )

    def pass_on(src, offset, part):
        for way in onward(offset, part):
            copy(src, part, peers[way], sends[part]).start()
            sends[part] += 1

    for part in range(3):
        pass_on(me, 0, part)
    swap = pltpu.make_async_remote_copy(
        src_ref=ow_ref, dst_ref=ow_out, send_sem=swap_sem.at[0], recv_sem=swap_sem.at[1],
        device_id=(me, 1 - core), device_id_type=MESH_ID,
    )

    qt[...] = jnp.zeros_like(qt)
    q_gain = column(qg_ref)
    for j in range(4):
        heads = turned_heads(
            lax.dot_general(
                order, q_ref[:, 128 * j : 128 * j + 128], nt, preferred_element_type=jnp.float32
            ),
            q_gain, cosine, sine,
        )
        for i in range(2):
            scaled = heads[i].astype(jnp.bfloat16).astype(jnp.float32) * QSCALE
            high = scaled.astype(jnp.bfloat16)
            low = (scaled - high.astype(jnp.float32)).astype(jnp.bfloat16)
            at, to = pl.ds((2 * j + i) * 256, 256), 64 * (j // 2)
            qt[to : to + 64, at] = high
            qt[128 + to : 192 + to, at] = low

    own = kv[me, 0:256, :]
    own = jnp.concatenate([own, own], axis=1)
    for t in range(4):
        at = pl.ds(t * 512, 512)
        s = jnp.dot(own, qt[:, at], preferred_element_type=jnp.float32)
        top[:, at] = jnp.broadcast_to(jnp.max(s, axis=0, keepdims=True), (8, 512))
    acc[...] = jnp.zeros_like(acc)
    ones = jnp.ones((16, 1024), jnp.bfloat16)

    words = packed()
    plan = relay_plan()

    def group(g, carry):
        for i, pieces in enumerate(plan):

            @pl.when(g == i)
            def _():
                for offset, part in pieces:
                    src = source_of(offset, me)
                    copy(src, part, me, 0).wait_recv()
                    pass_on(src, offset, part)
                if i == 1:
                    swap.start()

        now = lookup(words, g)
        srcs = [source_of((now // 64**j) % 64, me) for j in range(4)]
        for s in srcs:
            pltpu.make_async_copy(kv.at[s], kv_out.at[s], out_sem.at[s]).start()
        kk = jnp.concatenate([kv[s, 0:256, :] for s in srcs], axis=0)
        kk = jnp.concatenate([kk, kk], axis=1)
        vt = jnp.concatenate([kv[s, a : a + 128, :] for s in srcs for a in (256, 384)], axis=1)
        va = [jnp.concatenate([vt[64 * h : 64 * h + 64], ones], axis=0) for h in range(2)]
        for t in range(4):
            at = pl.ds(t * 512, 512)
            s = jnp.dot(kk, qt[:, at], preferred_element_type=jnp.float32)
            p = jnp.exp2(s - top[0:1, at]).astype(jnp.bfloat16)
            acc[:, at] += jnp.dot(va[t // 2], p, preferred_element_type=jnp.float32)
        return carry

    lax.fori_loop(0, 16, group, 0)

    for j in range(4):
        parts = []
        for i in range(2):
            at = pl.ds((2 * j + i) * 256, 256)
            parts.append(acc[0:64, at] / acc[64:65, at])
        o_ref[:, 128 * j : 128 * j + 128] = jnp.concatenate(parts, axis=0).T.astype(jnp.bfloat16)
    den_ref[0, 0] = jnp.max(acc[64:65, :])

    def drain(n, carry):
        for part in range(3):
            copy(me, part, me, n).wait_send()
        return carry

    def put_out(s, carry):
        pltpu.make_async_copy(kv.at[s], kv_out.at[s], out_sem.at[s]).wait()
        return carry

    lax.fori_loop(0, 63, drain, 0)
    lax.fori_loop(0, 64, put_out, 0)
    swap.wait()


def attention(queries, keys, values, q_gain, k_gain, out_weight):
    vmem, hbm = pl.BlockSpec(memory_space=pltpu.VMEM), pl.BlockSpec(memory_space=pltpu.HBM)
    return pl.pallas_call(
        attention_kernel,
        out_shape=(
            jax.ShapeDtypeStruct((256, 512), jnp.bfloat16),
            jax.ShapeDtypeStruct((1, 1), jnp.float32),
            jax.ShapeDtypeStruct((64, 512, 128), jnp.bfloat16),
            jax.ShapeDtypeStruct((512, 2048), jnp.bfloat16),
        ),
        in_specs=[vmem] * 5 + [hbm],
        out_specs=(vmem, pl.BlockSpec(memory_space=pltpu.SMEM), hbm, hbm),
        scratch_shapes=[
            pltpu.VMEM((256, 2048), jnp.bfloat16),
            pltpu.VMEM((8, 2048), jnp.float32),
            pltpu.VMEM((80, 2048), jnp.float32),
            pltpu.VMEM((64, 512, 128), jnp.bfloat16),
            pltpu.SemaphoreType.DMA((3, 63)),
            pltpu.SemaphoreType.DMA((3, 64)),
            pltpu.SemaphoreType.DMA((64,)),
            pltpu.SemaphoreType.DMA((2,)),
        ],
        compiler_params=pltpu.CompilerParams(
            collective_id=0, has_side_effects=True, vmem_limit_bytes=56 << 20
        ),
        cost_estimate=pl.CostEstimate(flops=17_000_000_000, bytes_accessed=9_000_000, transcendentals=0),
        name="attention",
    )(queries, keys, values, q_gain[None], k_gain[None], out_weight)


def attention_again(queries, q_gain, kv):
    me = lax.axis_index("sp")
    positions = me * 256 + jnp.arange(256, dtype=jnp.int32)
    qn = qk_prepare(queries, q_gain, positions, 8).reshape(256, 2, 4, 32, 2)
    qn = jnp.swapaxes(qn, -1, -2).reshape(256, 2, 4, 64)
    k = kv[:, 0:256].reshape(64, 256, 2, 64)
    v = jnp.concatenate([kv[:, 256:384], kv[:, 384:512]], axis=2).reshape(64, 2, 64, 256)

    def scores_of(kb):
        return jnp.einsum("qhgd,khd->hgqk", qn, kb, preferred_element_type=jnp.float32) * 0.125

    def largest(m, kb):
        return jnp.maximum(m, jnp.max(scores_of(kb), axis=-1)), None

    top, _ = lax.scan(largest, jnp.full((2, 4, 256), -1e30, jnp.float32), k)

    def add(carry, block):
        total, summed = carry
        kb, vb = block
        ex = jnp.exp(scores_of(kb) - top[..., None])
        summed += jnp.einsum(
            "hgqk,hdk->hgqd", ex.astype(jnp.bfloat16), vb, preferred_element_type=jnp.float32
        )
        return (total + jnp.sum(ex, axis=-1), summed), None

    zero = (jnp.zeros((2, 4, 256), jnp.float32), jnp.zeros((2, 4, 256, 64), jnp.float32))
    (total, summed), _ = lax.scan(add, zero, (k, v))
    out = jnp.transpose(summed / total[..., None], (2, 0, 1, 3))
    return out.reshape(256, 512).astype(jnp.bfloat16)


SLOTS = 6
PLANE = 16 * SLOTS
OWN = 10


def experts_kernel(
    att_ref, resid_ref, pg_ref, fg_ref, pfg_ref, ids_ref, rw_ref, ow_ref, owp_ref, gate_hbm, up_hbm, down_hbm, o_ref,
    ow, owp, gate, up, down, att_in, hidden, out, arr, x, inner, part, part_out, part_in, total, ret, combined, tiles,
    w_sem, a_sem, d_send, d_recv, f_send, f_recv, p_send, p_recv, r_send, r_recv,
):
    me, core = lax.axis_index("sp"), lax.axis_index("tp")
    other = 1 - core
    f32, bf16 = jnp.float32, jnp.bfloat16

    barrier = pltpu.get_barrier_semaphore()

    def greet(i, carry):
        pl.semaphore_signal(barrier, inc=1, device_id=((me + i) % 64, core), device_id_type=MESH_ID)
        return carry

    lax.fori_loop(1, 64, greet, 0)
    pl.semaphore_signal(barrier, inc=1, device_id=(me, other), device_id_type=MESH_ID)
    loads = [
        pltpu.make_async_copy(src, dst, w_sem.at[i])
        for i, (src, dst) in enumerate(
            ((ow_ref, ow), (owp_ref, owp), (gate_hbm.at[0], gate), (up_hbm.at[0], up), (down_hbm.at[0], down))
        )
    ]
    for load in loads:
        load.start()

    expert = lax.broadcasted_iota(jnp.int32, (64, 128), 0)
    chosen = [(ids_ref[k : k + 1, :] == expert).astype(f32) for k in range(2)]
    above = (
        lax.broadcasted_iota(jnp.int32, (128, 128), 0) < lax.broadcasted_iota(jnp.int32, (128, 128), 1)
    ).astype(f32).astype(bf16)
    earlier = [jnp.dot(c.astype(bf16), above, preferred_element_type=f32) for c in chosen]
    earlier[1] = earlier[1] + jnp.sum(chosen[0], axis=1, keepdims=True)
    slot = [
        ids_ref[k : k + 1, :] * SLOTS
        + jnp.sum(earlier[k] * chosen[k], axis=0, keepdims=True).astype(jnp.int32)
        for k in range(2)
    ]
    line = lax.broadcasted_iota(jnp.int32, (PLANE, 128), 0)
    member = (line * 43) // 256

    def offset_of(j, i):
        dz, dy = (i // 4 + 2) % 4, (i % 4 + 2) % 4
        return dz, dy, (j + 8 - dz - dy) % 4

    def chip_at(j, i, sign):
        dz, dy, dx = offset_of(j, i)
        cz = (me // 16 + 4 + sign * dz) % 4
        cy = ((me // 4) % 4 + 4 + sign * dy) % 4
        cx = (me % 4 + 4 + sign * dx) % 4
        return cz * 16 + cy * 4 + cx

    def place_of(j):
        return chip_at(j, member, 1) * SLOTS + line - member * SLOTS

    pl.semaphore_wait(barrier, 64)

    here = pl.ds(pl.multiple_of(core * 128, 128), 128)
    there = pl.ds(pl.multiple_of(other * 128, 128), 128)
    swap = pltpu.make_async_remote_copy(
        src_ref=att_ref.at[there], dst_ref=att_in, send_sem=a_sem.at[0], recv_sem=a_sem.at[1],
        device_id=(me, other), device_id_type=MESH_ID,
    )
    swap.start()
    loads[0].wait()
    mixed = jnp.dot(att_ref[here, :], ow[...], preferred_element_type=f32)
    loads[1].wait()
    swap.wait()
    mixed = mixed + jnp.dot(att_in[...], owp[...], preferred_element_type=f32)
    state = (resid_ref[...].astype(f32) + rms_scale(mixed, pg_ref[...])).astype(bf16)
    hidden[...] = state
    normed = rms_scale(state.astype(f32), fg_ref[...]).astype(bf16)

    def send(src, dst, number, sems, to):
        rows = pl.ds(number * SLOTS, SLOTS)
        return pltpu.make_async_remote_copy(
            src_ref=src.at[rows], dst_ref=dst.at[rows], send_sem=sems[0].at[number], recv_sem=sems[1].at[number],
            device_id=(to, core), device_id_type=MESH_ID,
        )

    def there_copy(j, i):
        return send(out, arr.at[core], j * 16 + i, (d_send, d_recv), chip_at(j, i, 1))

    def back_copy(j, i):
        return send(total, ret, j * 16 + i, (r_send, r_recv), chip_at(j, i, -1))

    def each(j, act):
        def step(i, carry):
            @pl.when(jnp.logical_or(j > 0, i != OWN))
            def _():
                act(j, i)

            return carry

        lax.fori_loop(0, 16, step, 0)

    own = pl.ds(OWN * SLOTS, SLOTS)

    def dispatch(j, carry):
        place = place_of(j)
        picked = ((slot[0] == place).astype(f32) + (slot[1] == place).astype(f32)).astype(bf16)
        rows = jnp.dot(picked, normed, preferred_element_type=f32)
        tiles[...] = rows.astype(bf16).reshape(PLANE, 16, 128)
        out[pl.ds(j * PLANE, PLANE)] = tiles[...]
        each(j, lambda j, i: there_copy(j, i).start())
        return carry

    lax.fori_loop(0, 4, dispatch, 0)
    arr[core, own] = out[own]
    for load in loads[2:]:
        load.wait()

    def forward(j):
        rows = pl.ds(j * PLANE, PLANE)
        return pltpu.make_async_remote_copy(
            src_ref=arr.at[core, rows], dst_ref=arr.at[core, rows], send_sem=f_send.at[j], recv_sem=f_recv.at[j],
            device_id=(me, other), device_id_type=MESH_ID,
        )

    def partial(j):
        return pltpu.make_async_remote_copy(
            src_ref=part_out.at[j], dst_ref=part_in.at[j], send_sem=p_send.at[j], recv_sem=p_recv.at[j],
            device_id=(me, other), device_id_type=MESH_ID,
        )

    def finish(j):
        partial(j).wait_recv()
        rows = (part[j].astype(f32) + part_in[j].astype(f32)).astype(bf16)
        tiles[...] = rows.reshape(PLANE, 16, 128)
        total[pl.ds(j * PLANE, PLANE)] = tiles[...]

        @pl.when(j == 0)
        def _():
            ret[own] = total[own]

        each(j, lambda j, i: back_copy(j, i).start())

    def chunk(j, carry):
        rows = pl.ds(j * PLANE, PLANE)
        each(j, lambda j, i: there_copy(j, i).wait_recv())
        forward(j).start()
        tiles[...] = arr[core, rows]
        x[0:PLANE, :] = tiles[...].reshape(PLANE, 2048)

        @pl.when(j > 0)
        def _():
            finish(j - 1)

        forward(j).wait_recv()
        tiles[...] = arr[other, rows]
        x[PLANE : 2 * PLANE, :] = tiles[...].reshape(PLANE, 2048)
        for n in range(7):
            at = pl.ds(n * 256, 256)
            g = jnp.dot(x[...], gate[:, at], preferred_element_type=f32)
            u = jnp.dot(x[...], up[:, at], preferred_element_type=f32)
            inner[:, at] = (g / (1.0 + jnp.exp(-g)) * u).astype(bf16)
        for n in range(8):
            at = pl.ds(n * 256, 256)
            y = jnp.dot(inner[...], down[:, at], preferred_element_type=f32).astype(bf16)
            part[j, :, at] = y[0:PLANE]
            part_out[j, :, at] = y[PLANE : 2 * PLANE]

        partial(j).start()
        return carry

    lax.fori_loop(0, 4, chunk, 0)
    finish(jnp.int32(3))

    combined[...] = jnp.zeros_like(combined)

    def collect(j, carry):
        each(j, lambda j, i: back_copy(j, i).wait_recv())
        place = place_of(j)
        weight = jnp.where(slot[0] == place, rw_ref[0:1, :], 0.0) + jnp.where(slot[1] == place, rw_ref[1:2, :], 0.0)
        high = weight.astype(bf16)
        low = (weight - high.astype(f32)).astype(bf16)
        tiles[...] = ret[pl.ds(j * PLANE, PLANE)]
        rows = tiles[...].reshape(PLANE, 2048)
        tn = (((0,), (0,)), ((), ()))
        combined[...] += lax.dot_general(high, rows, tn, preferred_element_type=f32) + lax.dot_general(
            low, rows, tn, preferred_element_type=f32
        )
        return carry

    lax.fori_loop(0, 4, collect, 0)
    o_ref[...] = (hidden[...].astype(f32) + rms_scale(combined[...], pfg_ref[...])).astype(bf16)

    def drain(j, carry):
        each(j, lambda j, i: there_copy(j, i).wait_send())
        each(j, lambda j, i: back_copy(j, i).wait_send())
        forward(j).wait_send()
        partial(j).wait_send()
        return carry

    lax.fori_loop(0, 4, drain, 0)


def experts(attended, resid, post_gain, ffn_gain, post_ffn_gain, route_ids, route_w, out_weight, out_weight_other, gate_w, up_w, down_w):
    vmem, hbm = pl.BlockSpec(memory_space=pltpu.VMEM), pl.BlockSpec(memory_space=pltpu.HBM)
    bf16, f32, dma = jnp.bfloat16, jnp.float32, pltpu.SemaphoreType.DMA
    return pl.pallas_call(
        experts_kernel,
        out_shape=jax.ShapeDtypeStruct((128, 2048), bf16),
        in_specs=[vmem] * 7 + [hbm] * 5,
        out_specs=vmem,
        scratch_shapes=[
            pltpu.VMEM((512, 2048), bf16),
            pltpu.VMEM((512, 2048), bf16),
            pltpu.VMEM((2048, 1792), bf16),
            pltpu.VMEM((2048, 1792), bf16),
            pltpu.VMEM((1792, 2048), bf16),
            pltpu.VMEM((128, 512), bf16),
            pltpu.VMEM((128, 2048), bf16),
            pltpu.VMEM((384, 16, 128), bf16),
            pltpu.VMEM((2, 384, 16, 128), bf16),
            pltpu.VMEM((2 * PLANE, 2048), bf16),
            pltpu.VMEM((2 * PLANE, 1792), bf16),
            pltpu.VMEM((4, PLANE, 2048), bf16),
            pltpu.VMEM((4, PLANE, 2048), bf16),
            pltpu.VMEM((4, PLANE, 2048), bf16),
            pltpu.VMEM((384, 16, 128), bf16),
            pltpu.VMEM((384, 16, 128), bf16),
            pltpu.VMEM((128, 2048), f32),
            pltpu.VMEM((PLANE, 16, 128), bf16),
            dma((5,)), dma((2,)), dma((64,)), dma((64,)), dma((4,)), dma((4,)), dma((4,)), dma((4,)),
            dma((64,)), dma((64,)),
        ],
        compiler_params=pltpu.CompilerParams(
            collective_id=1, has_side_effects=True, vmem_limit_bytes=60 << 20
        ),
        cost_estimate=pl.CostEstimate(flops=20_000_000_000, bytes_accessed=28_000_000, transcendentals=0),
        name="experts",
    )(
        attended, resid, post_gain[None], ffn_gain[None], post_ffn_gain[None], route_ids.T, route_w.T,
        out_weight, out_weight_other, gate_w, up_w, down_w,
    )


def per_device(
    queries,
    keys,
    values,
    q_gain,
    k_gain,
    resid,
    out_weight,
    post_gain,
    ffn_gain,
    post_ffn_gain,
    gate_w,
    up_w,
    down_w,
    route_ids,
    route_w,
):
    attended, den, kv, out_weight_other = attention(queries, keys, values, q_gain, k_gain, out_weight)
    attended = lax.cond(
        den[0, 0] < LIMIT,
        lambda: attended,
        lambda: attention_again(queries, q_gain, kv),
    )
    return experts(
        attended, resid, post_gain, ffn_gain, post_ffn_gain, route_ids, route_w, out_weight, out_weight_other,
        gate_w, up_w, down_w,
    )


def solution(mesh):
    in_specs = (
        P("sp", "tp"),
        P("sp", "tp"),
        P("sp", "tp"),
        P(),
        P(),
        P(("sp", "tp"), None),
        P("tp", None),
        P(),
        P(),
        P(),
        P("sp", None, "tp"),
        P("sp", None, "tp"),
        P("sp", "tp", None),
        P(("sp", "tp"), None),
        P(("sp", "tp"), None),
    )
    out_specs = P(("sp", "tp"), None)
    return jax.shard_map(
        per_device, mesh=mesh, in_specs=in_specs, out_specs=out_specs, check_vma=False
    )
```

time: 155 us -> 128 us (0.83)
  Pallas kernels: 144 us -> 125 us
  local copies, waits for them, and re-layouts: 7.62 us -> 1.89 us
  other arithmetic: 1.65 us -> 0 us
    pallas_call x1, Pallas kernels: 70.3 us -> 59.5 us  [attention(): pl.pallas_call(attention_kernel, out_shape=(jax.ShapeDtypeStruct((256, 51...]
    pallas_call x1, Pallas kernels: 73.4 us -> 65.2 us  [experts(): pl.pallas_call(experts_kernel, out_shape=jax.ShapeDtypeStruct((128, 2048)...]
    unnamed x17 -> x5, local copies, waits for them, and re-layouts: 3.78 us -> 1.89 us
    reshape x4 -> x0, local copies, waits for them, and re-layouts: 1.68 us -> none  [attention(): pairs = [g.reshape(32, 2).T.reshape(64) for g in (q_gain, k_gain)]]
where the time goes in v1:
time: 128 us; the launch traced here: 127 us
  Pallas kernels  125 us (98%)
  local copies, waits for them, and re-layouts  1.89 us (1%)
    pallas_call x1, Pallas kernels, experts(): pl.pallas_call(experts_kernel, out_shape=jax.ShapeDtypeStruct((128, 2048)...  65.2 us
    pallas_call x1, Pallas kernels, attention(): pl.pallas_call(attention_kernel, out_shape=(jax.ShapeDtypeStruct((256, 51...  59.5 us

profile of v1, /device:TPU:1, one launch (start us, length us, event | category | flops | bytes accessed | tf_op | source)
XLA Modules:
  0.0 127.5 jit_solution(14761377827476981274)
XLA Ops:
  0.0 0.0 copy-start
  0.0 0.0 copy-start.1
  0.0 59.5 %attention.1 = (bf16[256,512]{1,0:T(8,128)(2,1)S(1)}, f32[1,1]{1,0:T(1,128)}, bf16[64,512,128]{2,1,0:T(8,128)(2,1)}, bf16[512,2048]{1,0:T(8,128)(2,1)}) custom-call(bf16[256,512]{1,0:T(8,128)(2,1)} %q_ref.1, bf16[256,128]{1,0:T(8,128)(2,1)} %k_ref.1, bf16[256,128]{1,0:T(8,128)(2,1)} %v_ref.1, f32[1,64]{1,0:T(1,128)} %bitcast.75, f32[1,64]{1,0:T(1,128)} %bitcast.81, ...), custom_call_target="tpu_custom_call" | custom-call | flops 16999999488 | bytes 9000000 | tf_op jit(solution)/shard_map/attention/pallas_call | solution.py:251
  60.2 0.0 copy-done
  60.2 0.0 copy-done.1
  60.2 0.2 conditional.1
  60.4 65.2 %experts.1 = bf16[128,2048]{1,0:T(8,128)(2,1)} custom-call(bf16[256,512]{1,0:T(8,128)(2,1)S(1)} %get-tuple-element.128.att_ref, bf16[128,2048]{1,0:T(8,128)(2,1)} %resid_ref.1, f32[1,2048]{1,0:T(1,128)} %bitcast.76, f32[1,2048]{1,0:T(1,128)} %bitcast.77, f32[1,2048]{1,0:T(1,128)} %bitcast.78, s32[2,128]{1,0:T(2,128)} %bitcast.79, f32[2,128]{1,0:T(2,128)} %bitcast.80, ...), custom_call_target="tpu_custom_call" | custom-call | flops 20000000000 | bytes 28000000 | tf_op jit(solution)/shard_map/experts/pallas_call | solution.py:515
  125.6 1.9 %copy.51 = bf16[128,2048]{1,0:T(8,128)(2,1)} copy(bf16[128,2048]{1,0:T(8,128)(2,1)} %experts.1) | data formatting | bytes 1048576
Async XLA Ops:
  0.0 60.2 %copy-start = (bf16[256,512]{1,0:T(8,128)(2,1)S(1)}, bf16[256,512]{1,0:T(8,128)(2,1)}, u32[]{:S(2)}) copy-start(bf16[256,512]{1,0:T(8,128)(2,1)} %q_ref.1) | copy-start | bytes 786436
  0.0 60.2 %copy-start.1 = (f32[64]{0:T(128)S(1)}, f32[64]{0:T(128)}, u32[]{:S(2)}) copy-start(f32[64]{0:T(128)} %param.24) | copy-start | bytes 772

commit v2 on v1

--- a/solution.py
+++ b/solution.py
@@ -85,6 +85,10 @@
     cy = ((me // 4) % 4 + 4 - (offset // 4) % 4) % 4
     cx = (me % 4 + 4 - offset % 4) % 4
     return cz * 16 + cy * 4 + cx
+
+
+def rows_of(src, start, count):
+    return pl.ds(pl.multiple_of(src * 512 + start, 16), count)
 
 
 def turned_heads(x, gain, cosine, sine):
@@ -137,27 +141,35 @@
     kt = turned_heads(
         lax.dot_general(order, k_ref[...], nt, preferred_element_type=jnp.float32), column(kg_ref), cosine, sine
     )
-    kv[me, 0:256, :] = jnp.concatenate(kt, axis=0).T.astype(jnp.bfloat16)
+    kv[rows_of(me, 0, 256), :] = jnp.concatenate(kt, axis=0).T.astype(jnp.bfloat16)
     vt = lax.dot_general(same, v_ref[...], nt, preferred_element_type=jnp.float32).astype(jnp.bfloat16)
-    kv[me, 256:384, :] = vt[:, 0:128]
-    kv[me, 384:512, :] = vt[:, 128:256]
+    kv[rows_of(me, 256, 128), :] = vt[:, 0:128]
+    kv[rows_of(me, 384, 128), :] = vt[:, 128:256]
 
     pl.semaphore_wait(barrier, 7)
 
-    sends = [0, 0, 0]
-
-    def copy(src, part, to, number):
-        rows = pl.ds(*PARTS[part])
+    def copy(src, part, to, first):
+        rows = rows_of(src, *PARTS[part])
         return pltpu.make_async_remote_copy(
-            src_ref=kv.at[src, rows], dst_ref=kv.at[src, rows],
-            send_sem=send_sem.at[part, number], recv_sem=recv_sem.at[part, src],
+            src_ref=kv.at[rows], dst_ref=kv.at[rows],
+            send_sem=send_sem.at[part], recv_sem=recv_sem.at[part if first else 0, src],
             device_id=(to, core), device_id_type=MESH_ID,
+        )
+
+    def whole(src):
+        rows = rows_of(src, 0, 512)
+        return pltpu.make_async_remote_copy(
+            src_ref=kv.at[rows], dst_ref=kv.at[rows], send_sem=send_sem.at[0], recv_sem=recv_sem.at[0, src],
+            device_id=(me, core), device_id_type=MESH_ID,
         )
 
     def pass_on(src, offset, part):
         for way in onward(offset, part):
-            copy(src, part, peers[way], sends[part]).start()
-            sends[part] += 1
+            copy(src, part, peers[way], offset == 0).start()
+
+    def put_out(s):
+        rows = rows_of(s, 0, 512)
+        return pltpu.make_async_copy(kv.at[rows], kv_out.at[rows], out_sem.at[0])
 
     for part in range(3):
         pass_on(me, 0, part)
@@ -183,7 +195,7 @@
             qt[to : to + 64, at] = high
             qt[128 + to : 192 + to, at] = low
 
-    own = kv[me, 0:256, :]
+    own = kv[rows_of(me, 0, 256), :]
     own = jnp.concatenate([own, own], axis=1)
     for t in range(4):
         at = pl.ds(t * 512, 512)
@@ -202,7 +214,10 @@
             def _():
                 for offset, part in pieces:
                     src = source_of(offset, me)
-                    copy(src, part, me, 0).wait_recv()
+                    if i == 0:
+                        copy(src, part, me, True).wait_recv()
+                    elif part == 0:
+                        whole(src).wait_recv()
                     pass_on(src, offset, part)
                 if i == 1:
                     swap.start()
@@ -210,10 +225,10 @@
         now = lookup(words, g)
         srcs = [source_of((now // 64**j) % 64, me) for j in range(4)]
         for s in srcs:
-            pltpu.make_async_copy(kv.at[s], kv_out.at[s], out_sem.at[s]).start()
-        kk = jnp.concatenate([kv[s, 0:256, :] for s in srcs], axis=0)
+            put_out(s).start()
+        kk = jnp.concatenate([kv[rows_of(s, 0, 256), :] for s in srcs], axis=0)
         kk = jnp.concatenate([kk, kk], axis=1)
-        vt = jnp.concatenate([kv[s, a : a + 128, :] for s in srcs for a in (256, 384)], axis=1)
+        vt = jnp.concatenate([kv[rows_of(s, a, 128), :] for s in srcs for a in (256, 384)], axis=1)
         va = [jnp.concatenate([vt[64 * h : 64 * h + 64], ones], axis=0) for h in range(2)]
         for t in range(4):
             at = pl.ds(t * 512, 512)
@@ -232,17 +247,13 @@
         o_ref[:, 128 * j : 128 * j + 128] = jnp.concatenate(parts, axis=0).T.astype(jnp.bfloat16)
     den_ref[0, 0] = jnp.max(acc[64:65, :])
 
-    def drain(n, carry):
-        for part in range(3):
-            copy(me, part, me, n).wait_send()
-        return carry
-
-    def put_out(s, carry):
-        pltpu.make_async_copy(kv.at[s], kv_out.at[s], out_sem.at[s]).wait()
-        return carry
-
-    lax.fori_loop(0, 63, drain, 0)
-    lax.fori_loop(0, 64, put_out, 0)
+    for part in range(3):
+        sent = kv.at[pl.ds(0, 63 * PARTS[part][1])]
+        pltpu.make_async_remote_copy(
+            src_ref=sent, dst_ref=sent, send_sem=send_sem.at[part], recv_sem=recv_sem.at[part, 0],
+            device_id=(me, core), device_id_type=MESH_ID,
+        ).wait_send()
+    pltpu.make_async_copy(kv, kv_out, out_sem.at[0]).wait()
     swap.wait()
 
 
@@ -253,7 +264,7 @@
         out_shape=(
             jax.ShapeDtypeStruct((256, 512), jnp.bfloat16),
             jax.ShapeDtypeStruct((1, 1), jnp.float32),
-            jax.ShapeDtypeStruct((64, 512, 128), jnp.bfloat16),
+            jax.ShapeDtypeStruct((64 * 512, 128), jnp.bfloat16),
             jax.ShapeDtypeStruct((512, 2048), jnp.bfloat16),
         ),
         in_specs=[vmem] * 5 + [hbm],
@@ -262,10 +273,10 @@
             pltpu.VMEM((256, 2048), jnp.bfloat16),
             pltpu.VMEM((8, 2048), jnp.float32),
             pltpu.VMEM((80, 2048), jnp.float32),
-            pltpu.VMEM((64, 512, 128), jnp.bfloat16),
-            pltpu.SemaphoreType.DMA((3, 63)),
+            pltpu.VMEM((64 * 512, 128), jnp.bfloat16),
+            pltpu.SemaphoreType.DMA((3,)),
             pltpu.SemaphoreType.DMA((3, 64)),
-            pltpu.SemaphoreType.DMA((64,)),
+            pltpu.SemaphoreType.DMA((1,)),
             pltpu.SemaphoreType.DMA((2,)),
         ],
         compiler_params=pltpu.CompilerParams(
@@ -281,6 +292,7 @@
     positions = me * 256 + jnp.arange(256, dtype=jnp.int32)
     qn = qk_prepare(queries, q_gain, positions, 8).reshape(256, 2, 4, 32, 2)
     qn = jnp.swapaxes(qn, -1, -2).reshape(256, 2, 4, 64)
+    kv = kv.reshape(64, 512, 128)
     k = kv[:, 0:256].reshape(64, 256, 2, 64)
     v = jnp.concatenate([kv[:, 256:384], kv[:, 384:512]], axis=2).reshape(64, 2, 64, 256)
 
@@ -367,17 +379,17 @@
     def place_of(j):
         return chip_at(j, member, 1) * SLOTS + line - member * SLOTS
 
-    pl.semaphore_wait(barrier, 64)
-
     here = pl.ds(pl.multiple_of(core * 128, 128), 128)
     there = pl.ds(pl.multiple_of(other * 128, 128), 128)
+    loads[0].wait()
+    mixed = jnp.dot(att_ref[here, :], ow[...], preferred_element_type=f32)
+
+    pl.semaphore_wait(barrier, 64)
     swap = pltpu.make_async_remote_copy(
         src_ref=att_ref.at[there], dst_ref=att_in, send_sem=a_sem.at[0], recv_sem=a_sem.at[1],
         device_id=(me, other), device_id_type=MESH_ID,
     )
     swap.start()
-    loads[0].wait()
-    mixed = jnp.dot(att_ref[here, :], ow[...], preferred_element_type=f32)
     loads[1].wait()
     swap.wait()
     mixed = mixed + jnp.dot(att_in[...], owp[...], preferred_element_type=f32)
@@ -385,28 +397,37 @@
     hidden[...] = state
     normed = rms_scale(state.astype(f32), fg_ref[...]).astype(bf16)
 
-    def send(src, dst, number, sems, to):
-        rows = pl.ds(number * SLOTS, SLOTS)
+    def send(src, dst, j, rows, sems, to):
         return pltpu.make_async_remote_copy(
-            src_ref=src.at[rows], dst_ref=dst.at[rows], send_sem=sems[0].at[number], recv_sem=sems[1].at[number],
+            src_ref=src.at[rows], dst_ref=dst.at[rows], send_sem=sems[0].at[j], recv_sem=sems[1].at[j],
             device_id=(to, core), device_id_type=MESH_ID,
         )
 
+    def member_rows(j, i):
+        return pl.ds((j * 16 + i) * SLOTS, SLOTS)
+
     def there_copy(j, i):
-        return send(out, arr.at[core], j * 16 + i, (d_send, d_recv), chip_at(j, i, 1))
+        return send(out, arr.at[core], j, member_rows(j, i), (d_send, d_recv), chip_at(j, i, 1))
 
     def back_copy(j, i):
-        return send(total, ret, j * 16 + i, (r_send, r_recv), chip_at(j, i, -1))
+        return send(total, ret, j, member_rows(j, i), (r_send, r_recv), chip_at(j, i, -1))
 
     def each(j, act):
-        def step(i, carry):
-            @pl.when(jnp.logical_or(j > 0, i != OWN))
-            def _():
+        for i in range(16):
+            if i == OWN:
+                pl.when(j > 0)(lambda: act(j, OWN))
+            else:
                 act(j, i)
 
-            return carry
-
-        lax.fori_loop(0, 16, step, 0)
+    def all_there(j, count):
+        return send(out, arr.at[core], j, pl.ds(0, count * SLOTS), (d_send, d_recv), me)
+
+    def all_back(j, count):
+        return send(total, ret, j, pl.ds(0, count * SLOTS), (r_send, r_recv), me)
+
+    def once(j, act):
+        pl.when(j == 0)(lambda: act(15))
+        pl.when(j > 0)(lambda: act(16))
 
     own = pl.ds(OWN * SLOTS, SLOTS)
 
@@ -449,25 +470,40 @@
 
         each(j, lambda j, i: back_copy(j, i).start())
 
-    def chunk(j, carry):
+    def receive(j):
+        once(j, lambda count: all_there(j, count).wait_recv())
+        forward(j).start()
+
+    def unpack_own(j):
+        tiles[...] = arr[core, pl.ds(j * PLANE, PLANE)]
+        x[0:PLANE, :] = tiles[...].reshape(PLANE, 2048)
+
+    def unpack_other(j):
         rows = pl.ds(j * PLANE, PLANE)
-        each(j, lambda j, i: there_copy(j, i).wait_recv())
-        forward(j).start()
-        tiles[...] = arr[core, rows]
-        x[0:PLANE, :] = tiles[...].reshape(PLANE, 2048)
-
-        @pl.when(j > 0)
-        def _():
-            finish(j - 1)
-
         forward(j).wait_recv()
         tiles[...] = arr[other, rows]
         x[PLANE : 2 * PLANE, :] = tiles[...].reshape(PLANE, 2048)
+
+    receive(jnp.int32(0))
+    unpack_own(jnp.int32(0))
+    unpack_other(jnp.int32(0))
+
+    def chunk(j, carry):
         for n in range(7):
             at = pl.ds(n * 256, 256)
             g = jnp.dot(x[...], gate[:, at], preferred_element_type=f32)
             u = jnp.dot(x[...], up[:, at], preferred_element_type=f32)
             inner[:, at] = (g / (1.0 + jnp.exp(-g)) * u).astype(bf16)
+
+        @pl.when(j > 0)
+        def _():
+            finish(j - 1)
+
+        @pl.when(j < 3)
+        def _():
+            receive(j + 1)
+
+        unpack_own(jnp.minimum(j + 1, 3))
         for n in range(8):
             at = pl.ds(n * 256, 256)
             y = jnp.dot(inner[...], down[:, at], preferred_element_type=f32).astype(bf16)
@@ -475,6 +511,11 @@
             part_out[j, :, at] = y[PLANE : 2 * PLANE]
 
         partial(j).start()
+
+        @pl.when(j < 3)
+        def _():
+            unpack_other(j + 1)
+
         return carry
 
     lax.fori_loop(0, 4, chunk, 0)
@@ -483,7 +524,7 @@
     combined[...] = jnp.zeros_like(combined)
 
     def collect(j, carry):
-        each(j, lambda j, i: back_copy(j, i).wait_recv())
+        once(j, lambda count: all_back(j, count).wait_recv())
         place = place_of(j)
         weight = jnp.where(slot[0] == place, rw_ref[0:1, :], 0.0) + jnp.where(slot[1] == place, rw_ref[1:2, :], 0.0)
         high = weight.astype(bf16)
@@ -500,8 +541,8 @@
     o_ref[...] = (hidden[...].astype(f32) + rms_scale(combined[...], pfg_ref[...])).astype(bf16)
 
     def drain(j, carry):
-        each(j, lambda j, i: there_copy(j, i).wait_send())
-        each(j, lambda j, i: back_copy(j, i).wait_send())
+        once(j, lambda count: all_there(j, count).wait_send())
+        once(j, lambda count: all_back(j, count).wait_send())
         forward(j).wait_send()
         partial(j).wait_send()
         return carry
@@ -536,11 +577,11 @@
             pltpu.VMEM((384, 16, 128), bf16),
             pltpu.VMEM((128, 2048), f32),
             pltpu.VMEM((PLANE, 16, 128), bf16),
-            dma((5,)), dma((2,)), dma((64,)), dma((64,)), dma((4,)), dma((4,)), dma((4,)), dma((4,)),
-            dma((64,)), dma((64,)),
+            dma((5,)), dma((2,)), dma((4,)), dma((4,)), dma((4,)), dma((4,)), dma((4,)), dma((4,)),
+            dma((4,)), dma((4,)),
         ],
         compiler_params=pltpu.CompilerParams(
-            collective_id=1, has_side_effects=True, vmem_limit_bytes=60 << 20
+            collective_id=1, has_side_effects=True, vmem_limit_bytes=62 << 20
         ),
         cost_estimate=pl.CostEstimate(flops=20_000_000_000, bytes_accessed=28_000_000, transcendentals=0),
         name="experts",

time: 128 us -> 118 us (0.922)
  Pallas kernels: 125 us -> 115 us
    pallas_call x1, Pallas kernels: 65.2 us -> 58.2 us  [experts(): pl.pallas_call(experts_kernel, out_shape=jax.ShapeDtypeStruct((128, 2048)...]
    pallas_call x1, Pallas kernels: 59.5 us -> 56.3 us  [attention(): pl.pallas_call(attention_kernel, out_shape=(jax.ShapeDtypeStruct((256, 51...]
where the time goes in v2:
time: 118 us; the launch traced here: 117 us
  Pallas kernels  115 us (97%)
  local copies, waits for them, and re-layouts  1.89 us (2%)
    pallas_call x1, Pallas kernels, experts(): pl.pallas_call(experts_kernel, out_shape=jax.ShapeDtypeStruct((128, 2048)...  58.2 us
    pallas_call x1, Pallas kernels, attention(): pl.pallas_call(attention_kernel, out_shape=(jax.ShapeDtypeStruct((256, 51...  56.3 us

profile of v2, /device:TPU:1, one launch (start us, length us, event | category | flops | bytes accessed | tf_op | source)
XLA Modules:
  0.0 117.3 jit_solution(14612395939362500997)
XLA Ops:
  0.0 0.0 copy-start
  0.0 0.0 copy-start.1
  0.0 56.3 %attention.1 = (bf16[256,512]{1,0:T(8,128)(2,1)S(1)}, f32[1,1]{1,0:T(1,128)}, bf16[32768,128]{1,0:T(8,128)(2,1)}, bf16[512,2048]{1,0:T(8,128)(2,1)}) custom-call(bf16[256,512]{1,0:T(8,128)(2,1)} %q_ref.1, bf16[256,128]{1,0:T(8,128)(2,1)} %k_ref.1, bf16[256,128]{1,0:T(8,128)(2,1)} %v_ref.1, f32[1,64]{1,0:T(1,128)} %bitcast.78, f32[1,64]{1,0:T(1,128)} %bitcast.84, ...), custom_call_target="tpu_custom_call" | custom-call | flops 16999999488 | bytes 9000000 | tf_op jit(solution)/shard_map/attention/pallas_call | solution.py:262
  57.0 0.0 copy-done
  57.0 0.0 copy-done.1
  57.0 0.2 conditional.1
  57.2 58.2 %experts.1 = bf16[128,2048]{1,0:T(8,128)(2,1)} custom-call(bf16[256,512]{1,0:T(8,128)(2,1)S(1)} %get-tuple-element.128.att_ref, bf16[128,2048]{1,0:T(8,128)(2,1)} %resid_ref.1, f32[1,2048]{1,0:T(1,128)} %bitcast.79, f32[1,2048]{1,0:T(1,128)} %bitcast.80, f32[1,2048]{1,0:T(1,128)} %bitcast.81, s32[2,128]{1,0:T(2,128)} %bitcast.82, f32[2,128]{1,0:T(2,128)} %bitcast.83, ...), custom_call_target="tpu_custom_call" | custom-call | flops 20000000000 | bytes 28000000 | tf_op jit(solution)/shard_map/experts/pallas_call | solution.py:556
  115.4 1.9 %copy.51 = bf16[128,2048]{1,0:T(8,128)(2,1)} copy(bf16[128,2048]{1,0:T(8,128)(2,1)} %experts.1) | data formatting | bytes 1048576
Async XLA Ops:
  0.0 57.0 %copy-start = (bf16[256,512]{1,0:T(8,128)(2,1)S(1)}, bf16[256,512]{1,0:T(8,128)(2,1)}, u32[]{:S(2)}) copy-start(bf16[256,512]{1,0:T(8,128)(2,1)} %q_ref.1) | copy-start | bytes 786436
  0.0 57.0 %copy-start.1 = (f32[64]{0:T(128)S(1)}, f32[64]{0:T(128)}, u32[]{:S(2)}) copy-start(f32[64]{0:T(128)} %param.24) | copy-start | bytes 772

commit v3 on v2

--- a/solution.py
+++ b/solution.py
@@ -230,11 +230,11 @@
         kk = jnp.concatenate([kk, kk], axis=1)
         vt = jnp.concatenate([kv[rows_of(s, a, 128), :] for s in srcs for a in (256, 384)], axis=1)
         va = [jnp.concatenate([vt[64 * h : 64 * h + 64], ones], axis=0) for h in range(2)]
-        for t in range(4):
-            at = pl.ds(t * 512, 512)
+        for t in range(2):
+            at = pl.ds(t * 1024, 1024)
             s = jnp.dot(kk, qt[:, at], preferred_element_type=jnp.float32)
             p = jnp.exp2(s - top[0:1, at]).astype(jnp.bfloat16)
-            acc[:, at] += jnp.dot(va[t // 2], p, preferred_element_type=jnp.float32)
+            acc[:, at] += jnp.dot(va[t], p, preferred_element_type=jnp.float32)
         return carry
 
     lax.fori_loop(0, 16, group, 0)
@@ -489,15 +489,20 @@
     unpack_other(jnp.int32(0))
 
     def chunk(j, carry):
-        for n in range(7):
-            at = pl.ds(n * 256, 256)
-            g = jnp.dot(x[...], gate[:, at], preferred_element_type=f32)
-            u = jnp.dot(x[...], up[:, at], preferred_element_type=f32)
-            inner[:, at] = (g / (1.0 + jnp.exp(-g)) * u).astype(bf16)
+        def widen(first, end):
+            for n in range(first, end):
+                at = pl.ds(n * 256, 256)
+                g = jnp.dot(x[...], gate[:, at], preferred_element_type=f32)
+                u = jnp.dot(x[...], up[:, at], preferred_element_type=f32)
+                inner[:, at] = (g / (1.0 + jnp.exp(-g)) * u).astype(bf16)
+
+        widen(0, 3)
 
         @pl.when(j > 0)
         def _():
             finish(j - 1)
+
+        widen(3, 7)
 
         @pl.when(j < 3)
         def _():

time: 118 us -> 117 us (level)
  no operation moved by 1% of the time
where the time goes in v3:
time: 117 us
  Pallas kernels  114 us (97%)
  local copies, waits for them, and re-layouts  1.89 us (2%)
    pallas_call x1, Pallas kernels, experts(): pl.pallas_call(experts_kernel, out_shape=jax.ShapeDtypeStruct((128, 2048)...  57.8 us
    pallas_call x1, Pallas kernels, attention(): pl.pallas_call(attention_kernel, out_shape=(jax.ShapeDtypeStruct((256, 51...  56 us

profile of v3, /device:TPU:1, one launch (start us, length us, event | category | flops | bytes accessed | tf_op | source)
XLA Modules:
  0.0 116.7 jit_solution(11801274866929225772)
XLA Ops:
  0.0 0.0 copy-start
  0.0 0.0 copy-start.1
  0.0 56.0 %attention.1 = (bf16[256,512]{1,0:T(8,128)(2,1)S(1)}, f32[1,1]{1,0:T(1,128)}, bf16[32768,128]{1,0:T(8,128)(2,1)}, bf16[512,2048]{1,0:T(8,128)(2,1)}) custom-call(bf16[256,512]{1,0:T(8,128)(2,1)} %q_ref.1, bf16[256,128]{1,0:T(8,128)(2,1)} %k_ref.1, bf16[256,128]{1,0:T(8,128)(2,1)} %v_ref.1, f32[1,64]{1,0:T(1,128)} %bitcast.78, f32[1,64]{1,0:T(1,128)} %bitcast.84, ...), custom_call_target="tpu_custom_call" | custom-call | flops 16999999488 | bytes 9000000 | tf_op jit(solution)/shard_map/attention/pallas_call | solution.py:262
  56.7 0.0 copy-done
  56.7 0.0 copy-done.1
  56.7 0.2 conditional.1
  56.9 57.8 %experts.1 = bf16[128,2048]{1,0:T(8,128)(2,1)} custom-call(bf16[256,512]{1,0:T(8,128)(2,1)S(1)} %get-tuple-element.128.att_ref, bf16[128,2048]{1,0:T(8,128)(2,1)} %resid_ref.1, f32[1,2048]{1,0:T(1,128)} %bitcast.79, f32[1,2048]{1,0:T(1,128)} %bitcast.80, f32[1,2048]{1,0:T(1,128)} %bitcast.81, s32[2,128]{1,0:T(2,128)} %bitcast.82, f32[2,128]{1,0:T(2,128)} %bitcast.83, ...), custom_call_target="tpu_custom_call" | custom-call | flops 20000000000 | bytes 28000000 | tf_op jit(solution)/shard_map/experts/pallas_call | solution.py:561
  114.8 1.9 %copy.51 = bf16[128,2048]{1,0:T(8,128)(2,1)} copy(bf16[128,2048]{1,0:T(8,128)(2,1)} %experts.1) | data formatting | bytes 1048576
Async XLA Ops:
  0.0 56.7 %copy-start = (bf16[256,512]{1,0:T(8,128)(2,1)S(1)}, bf16[256,512]{1,0:T(8,128)(2,1)}, u32[]{:S(2)}) copy-start(bf16[256,512]{1,0:T(8,128)(2,1)} %q_ref.1) | copy-start | bytes 786436
  0.0 56.7 %copy-start.1 = (f32[64]{0:T(128)S(1)}, f32[64]{0:T(128)}, u32[]{:S(2)}) copy-start(f32[64]{0:T(128)} %param.24) | copy-start | bytes 772
